TPU v7x, 32 devices: a whole 2x2x4 slice. The times are simulated.
32 devices in a mesh: fs: 4 (over z), tp: 8 (over y, x, core).
Axes of the slice: x: 2, y: 2, z: 4, core: 2. Of those that a mesh axis runs over, the one named last changes fastest.
Arguments:
- grad_gate: float32 [2112, 5632], P('fs', 'tp'), may hold values from -45 to 45
- grad_up: float32 [2112, 5632], P('fs', 'tp'), may hold values from -45 to 45
- moment_gate: float32 [2112, 5632], P('fs', 'tp'), may hold values from -6 to 6
- moment_up: float32 [2112, 5632], P('fs', 'tp'), may hold values from -6 to 6
Outputs:
- moment_gate_next: float32 [2112, 5632], P('fs', 'tp')
- moment_up_next: float32 [2112, 5632], P('fs', 'tp')
- update_gate: float32 [2112, 5632], P('fs', 'tp')
- update_up: float32 [2112, 5632], P('fs', 'tp')
All inputs are finite; a program needn't handle non-finite values.
Results may differ from a plain program's by a relative error of at most 0.0019.
The roundings to bfloat16 on the way count: a program that leaves them out, or rounds other values in their place, can miss the bound.
Values may be sent and summed in bfloat16 or wider, within the bound.
A program may use at most 64 MiB of HBM per device.

v0:
```python
import jax
import jax.numpy as jnp
from jax import lax
from jax.sharding import PartitionSpec as P

FF = 5632
ITERS = 3
BETA = 0.95
EPS = 1e-06


def multiply(left_low, right_low):
    left_rows = lax.all_gather(left_low, "fs", axis=1, tiled=True)
    return jnp.dot(
        left_rows,
        lax.all_gather(right_low, "tp", axis=0, tiled=True),
        preferred_element_type=jnp.float32,
    )


def local(grad_gate, grad_up, moment_gate, moment_up):
    moment_gate_next = BETA * moment_gate + grad_gate
    moment_up_next = BETA * moment_up + grad_up
    low_gate = moment_gate_next.astype(jnp.bfloat16)
    low_up = moment_up_next.astype(jnp.bfloat16)
    trace_local = jnp.sum(jnp.square(low_gate.astype(jnp.float32))) + jnp.sum(
        jnp.square(low_up.astype(jnp.float32))
    )
    columns_gate, columns_up = (
        lax.all_gather(low_gate, "fs", axis=0, tiled=True),
        lax.all_gather(low_up, "fs", axis=0, tiled=True),
    )
    rows_dev = low_gate.shape[0]
    width = columns_gate.shape[0]
    own_rows = width // lax.axis_size("tp")
    block_gate = columns_gate
    block_up = columns_up
    gram = lax.psum_scatter(
        jnp.einsum("ik,jk->ij", block_gate, low_gate, preferred_element_type=jnp.float32)
        + jnp.einsum("ik,jk->ij", block_up, low_up, preferred_element_type=jnp.float32),
        "tp",
        scatter_dimension=0,
        tiled=True,
    )
    square_local = jnp.sum(gram * gram)
    trace_total, square_total = lax.psum((trace_local, square_local), ("fs", "tp"))
    spectral = 2.0 * square_total / (trace_total + EPS)
    current = gram / spectral
    row_index = lax.axis_index("tp") * own_rows + lax.broadcasted_iota(
        jnp.int32, (own_rows, rows_dev), 0
    )
    col_index = lax.axis_index("fs") * rows_dev + lax.broadcasted_iota(
        jnp.int32, (own_rows, rows_dev), 1
    )
    identity = (row_index == col_index).astype(jnp.float32)
    product_low = None
    for iteration in range(ITERS):
        poly_low = (1.5 * identity - 0.5 * current).astype(jnp.bfloat16)
        final_turn = iteration == ITERS - 1
        square_low = None
        if iteration == 0:
            product_low = poly_low
            square_low = multiply(poly_low, poly_low).astype(jnp.bfloat16)
        elif final_turn:
            product_low = multiply(product_low, poly_low).astype(jnp.bfloat16)
        else:
            product_low = multiply(product_low, poly_low).astype(jnp.bfloat16)
            square_low = multiply(poly_low, poly_low).astype(jnp.bfloat16)
        if not final_turn:
            current = multiply(current.astype(jnp.bfloat16), square_low)
    factor = jnp.sqrt(2.0 * FF / spectral)
    segment = lax.all_gather(product_low, "tp", axis=0, tiled=True)
    block_gate = columns_gate
    block_up = columns_up
    ortho_gate = jnp.einsum("jr,jc->rc", segment, block_gate, preferred_element_type=jnp.float32)
    ortho_up = jnp.einsum("jr,jc->rc", segment, block_up, preferred_element_type=jnp.float32)
    return (moment_gate_next, moment_up_next, ortho_gate * factor, ortho_up * factor)


def solution(mesh):
    in_specs = (P("fs", "tp"), P("fs", "tp"), P("fs", "tp"), P("fs", "tp"))
    out_specs = (P("fs", "tp"), P("fs", "tp"), P("fs", "tp"), P("fs", "tp"))
    return jax.shard_map(local, mesh=mesh, in_specs=in_specs, out_specs=out_specs, check_vma=False)
```

profile of v0, /device:TPU:0, one launch (start us, length us, event | category | flops | bytes accessed | tf_op | source)
XLA Modules:
  0.0 640.1 jit_solution(17345301320345391013)
XLA Ops:
  7.2 4.4 multiply_reduce_fusion.1
  11.7 4.0 multiply_reduce_fusion
  15.8 63.8 %all-gather.19.cloned.1.call-done = bf16[2112,704]{1,0:T(8,128)(2,1)} async-done(((bf16[528,704]{1,0:T(8,128)(2,1)}), bf16[2112,704]{1,0:T(8,128)(2,1)}) %all-gather.19.cloned.1.call-update) | async-done | bytes 2973712 | tf_op jit(solution)/shard_map/all_gather | solution.py:30
  79.6 7.0 %fusion.5 = f32[2112,528]{1,0:T(8,128)} fusion(bf16[2112,704]{1,0:T(8,128)(2,1)} %all-gather.19.cloned.1.call-done, bf16[528,704]{1,0:T(8,128)(2,1)S(1)} %copy-done), kind=kOutput, calls=%fused_computation.25 | convolution fusion | flops 1570111488 | bytes 8177664 | tf_op jit(solution)/shard_map/ik,jk->ij/dot_general | solution.py:39
  86.6 58.9 %all-gather.21.cloned.1.call-done = bf16[2112,704]{1,0:T(8,128)(2,1)} async-done(((bf16[528,704]{1,0:T(8,128)(2,1)}), bf16[2112,704]{1,0:T(8,128)(2,1)}) %all-gather.21.cloned.1.call-update) | async-done | bytes 2973712 | tf_op jit(solution)/shard_map/all_gather | solution.py:31
  145.5 8.6 %convolution_add_fusion = f32[2112,528]{1,0:T(8,128)} fusion(f32[2112,528]{1,0:T(8,128)} %fusion.5, bf16[2112,704]{1,0:T(8,128)(2,1)} %all-gather.21.cloned.1.call-done, bf16[528,704]{1,0:T(8,128)(2,1)S(1)} %copy-done.1), kind=kOutput, calls=%fused_computation | convolution fusion | flops 1571226624 | bytes 12638208 | tf_op jit(solution)/shard_map/ik,jk->ij/dot_general | solution.py:40
  155.4 54.1 %reduce-scatter.4.cloned.1.call-done = f32[264,528]{1,0:T(8,128)} async-done(((f32[2112,528]{1,0:T(8,128)}), f32[264,528]{1,0:T(8,128)}) %reduce-scatter.4.cloned.1.call-update) | async-done | bytes 557584
  209.5 1.9 multiply_reduce_fusion.2
  211.4 39.5 %all-reduce.1 = (f32[]{:T(128)}, f32[]{:T(128)}) all-reduce(f32[]{:T(128)} %multiply_reduce_fusion.2, f32[]{:T(128)S(6)} %add.42), channel_id=1, replica_groups=mesh['fs'=4,'tp'=8] {'fs','tp'}, use_global_device_ids=true, to_apply=%region_2.0 | all-reduce | flops 2 | bytes 16 | tf_op jit(solution)/shard_map/psum | solution.py:46
  252.2 2.1 convert_bitcast_fusion.1
  255.6 33.1 %all-gather.35.cloned.1.call-done = bf16[4,528,264]{1,2,0:T(8,128)(2,1)} async-done(((bf16[1,528,264]{1,2,0:T(8,128)(2,1)}), bf16[4,528,264]{1,2,0:T(8,128)(2,1)}) %all-gather.35.cloned.1.call-update) | async-done | bytes 1115152 | tf_op jit(solution)/shard_map/all_gather | solution.py:13
  288.6 1.9 copy.13
  291.3 29.0 %all-gather.23.cloned.1.call-done = bf16[2112,528]{1,0:T(8,128)(2,1)} async-done(((bf16[264,528]{1,0:T(8,128)(2,1)}), bf16[2112,528]{1,0:T(8,128)(2,1)}) %all-gather.23.cloned.1.call-update) | async-done | bytes 2230288 | tf_op jit(solution)/shard_map/all_gather | solution.py:16
  320.4 3.6 convolution_convert_fusion.3
  324.2 31.4 %all-gather.37.cloned.1.call-done = bf16[4,528,264]{1,2,0:T(8,128)(2,1)} async-done(((bf16[1,528,264]{1,2,0:T(8,128)(2,1)}), bf16[4,528,264]{1,2,0:T(8,128)(2,1)}) %all-gather.37.cloned.1.call-update) | async-done | bytes 1115152 | tf_op jit(solution)/shard_map/all_gather | solution.py:13
  355.6 1.9 copy.14
  359.3 28.2 %all-gather.25.cloned.1.call-done = bf16[2112,528]{1,0:T(8,128)(2,1)} async-done(((bf16[264,528]{1,0:T(8,128)(2,1)}), bf16[2112,528]{1,0:T(8,128)(2,1)}) %all-gather.25.cloned.1.call-update) | async-done | bytes 2230288 | tf_op jit(solution)/shard_map/all_gather | solution.py:16
  387.5 4.1 convert_bitcast_fusion
  393.0 32.0 %all-gather.43.cloned.1.call-done = bf16[4,528,264]{1,2,0:T(8,128)(2,1)} async-done(((bf16[1,528,264]{1,2,0:T(8,128)(2,1)}), bf16[4,528,264]{1,2,0:T(8,128)(2,1)}) %all-gather.43.cloned.1.call-update) | async-done | bytes 1115152 | tf_op jit(solution)/shard_map/all_gather | solution.py:13
  425.0 1.9 copy.17
  428.7 27.6 %all-gather.27.cloned.1.call-done = bf16[2112,528]{1,0:T(8,128)(2,1)} async-done(((bf16[264,528]{1,0:T(8,128)(2,1)}), bf16[2112,528]{1,0:T(8,128)(2,1)}) %all-gather.27.cloned.1.call-update) | async-done | bytes 2230288 | tf_op jit(solution)/shard_map/all_gather | solution.py:16
  456.3 4.0 convolution_convert_fusion.1
  460.3 3.6 fusion.2
  464.0 27.5 %all-gather.41.cloned.1.call-done = bf16[4,528,264]{1,2,0:T(8,128)(2,1)} async-done(((bf16[1,528,264]{1,2,0:T(8,128)(2,1)}), bf16[4,528,264]{1,2,0:T(8,128)(2,1)}) %all-gather.41.cloned.1.call-update) | async-done | bytes 1115152 | tf_op jit(solution)/shard_map/all_gather | solution.py:13
  494.2 28.6 %all-gather.29.cloned.1.call-done = bf16[2112,528]{1,0:T(8,128)(2,1)} async-done(((bf16[264,528]{1,0:T(8,128)(2,1)}), bf16[2112,528]{1,0:T(8,128)(2,1)}) %all-gather.29.cloned.1.call-update) | async-done | bytes 2230288 | tf_op jit(solution)/shard_map/all_gather | solution.py:16
  522.9 3.6 fusion.1
  526.8 31.3 %all-gather.39.cloned.1.call-done = bf16[4,528,264]{1,2,0:T(8,128)(2,1)} async-done(((bf16[1,528,264]{1,2,0:T(8,128)(2,1)}), bf16[4,528,264]{1,2,0:T(8,128)(2,1)}) %all-gather.39.cloned.1.call-update) | async-done | bytes 1115152 | tf_op jit(solution)/shard_map/all_gather | solution.py:13
  560.8 29.2 %all-gather.31.cloned.1.call-done = bf16[2112,528]{1,0:T(8,128)(2,1)} async-done(((bf16[264,528]{1,0:T(8,128)(2,1)}), bf16[2112,528]{1,0:T(8,128)(2,1)}) %all-gather.31.cloned.1.call-update) | async-done | bytes 2230288 | tf_op jit(solution)/shard_map/all_gather | solution.py:16
  590.0 3.6 convolution_convert_fusion
  593.7 30.4 %all-gather.33.cloned.1.call-done = bf16[2112,528]{1,0:T(8,128)(2,1)} async-done(((bf16[264,528]{1,0:T(8,128)(2,1)}), bf16[2112,528]{1,0:T(8,128)(2,1)}) %all-gather.33.cloned.1.call-update) | async-done | bytes 2230288 | tf_op jit(solution)/shard_map/all_gather | solution.py:72
  624.1 6.1 convolution_multiply_fusion
  630.2 3.3 convolution_multiply_fusion.1
  (47 shorter events, 13.3 us)
Async XLA Ops:
  7.2 72.4 %all-gather.19.cloned.1.call-start = ((), (), s32[]{:S(2)}) async-start(), calls=%async_computation.1 | async-start | bytes 4055040 | tf_op jit(solution)/shard_map/all_gather | solution.py:30
  7.2 4.5 copy-start.2
  11.7 67.9 %copy-start = (bf16[528,704]{1,0:T(8,128)(2,1)S(1)}, bf16[528,704]{1,0:T(8,128)(2,1)}, u32[]{:S(2)}) copy-start(bf16[528,704]{1,0:T(8,128)(2,1)} %get-tuple-element.10) | copy-start | bytes 2230276
  11.7 133.8 %all-gather.21.cloned.1.call-start = ((), (), s32[]{:S(2)}) async-start(), calls=%async_computation.2 | async-start | bytes 4055040 | tf_op jit(solution)/shard_map/all_gather | solution.py:31
  15.7 129.8 %copy-start.1 = (bf16[528,704]{1,0:T(8,128)(2,1)S(1)}, bf16[528,704]{1,0:T(8,128)(2,1)}, u32[]{:S(2)}) copy-start(bf16[528,704]{1,0:T(8,128)(2,1)} %get-tuple-element.7) | copy-start | bytes 2230276
  15.7 193.8 %reduce-scatter.4.cloned.1.call-start = ((), (), s32[]{:S(2)}) async-start(), calls=%async_computation.14 | async-start | bytes 6082560
  154.1 134.5 %all-gather.35.cloned.1.call-start = ((), (), s32[]{:S(2)}) async-start(), calls=%async_computation.9 | async-start | bytes 1689600 | tf_op jit(solution)/shard_map/all_gather | solution.py:13
  254.3 66.0 %all-gather.23.cloned.1.call-start = ((), (), s32[]{:S(2)}) async-start(), calls=%async_computation.3 | async-start | bytes 3041280 | tf_op jit(solution)/shard_map/all_gather | solution.py:16
  254.9 100.7 %all-gather.37.cloned.1.call-start = ((), (), s32[]{:S(2)}) async-start(), calls=%async_computation.10 | async-start | bytes 1689600 | tf_op jit(solution)/shard_map/all_gather | solution.py:13
  255.5 132.0 %all-gather.25.cloned.1.call-start = ((), (), s32[]{:S(2)}) async-start(), calls=%async_computation.4 | async-start | bytes 3041280 | tf_op jit(solution)/shard_map/all_gather | solution.py:16
  324.0 101.0 %all-gather.43.cloned.1.call-start = ((), (), s32[]{:S(2)}) async-start(), calls=%async_computation.13 | async-start | bytes 1689600 | tf_op jit(solution)/shard_map/all_gather | solution.py:13
  391.6 64.7 %all-gather.27.cloned.1.call-start = ((), (), s32[]{:S(2)}) async-start(), calls=%async_computation.5 | async-start | bytes 3041280 | tf_op jit(solution)/shard_map/all_gather | solution.py:16
  392.4 99.2 %all-gather.41.cloned.1.call-start = ((), (), s32[]{:S(2)}) async-start(), calls=%async_computation.12 | async-start | bytes 1689600 | tf_op jit(solution)/shard_map/all_gather | solution.py:13
  392.9 129.9 %all-gather.29.cloned.1.call-start = ((), (), s32[]{:S(2)}) async-start(), calls=%async_computation.6 | async-start | bytes 3041280 | tf_op jit(solution)/shard_map/all_gather | solution.py:16
  460.3 97.8 %all-gather.39.cloned.1.call-start = ((), (), s32[]{:S(2)}) async-start(), calls=%async_computation.11 | async-start | bytes 1689600 | tf_op jit(solution)/shard_map/all_gather | solution.py:13
  464.0 126.0 %all-gather.31.cloned.1.call-start = ((), (), s32[]{:S(2)}) async-start(), calls=%async_computation.7 | async-start | bytes 3041280 | tf_op jit(solution)/shard_map/all_gather | solution.py:16
  526.5 97.6 %all-gather.33.cloned.1.call-start = ((), (), s32[]{:S(2)}) async-start(), calls=%async_computation.8 | async-start | bytes 3041280 | tf_op jit(solution)/shard_map/all_gather | solution.py:72
  593.7 36.5 %copy-start.3 = (bf16[2112,704]{1,0:T(8,128)(2,1)S(1)}, bf16[2112,704]{1,0:T(8,128)(2,1)}, u32[]{:S(2)}) copy-start(bf16[2112,704]{1,0:T(8,128)(2,1)} %all-gather.19.cloned.1.call-done) | copy-start | bytes 8921092
  624.1 6.1 copy-start.4
Sparse Core Ops, SparseCore 0:
  11.8 67.7 all-gather.18
  81.7 63.6 all-gather.20
  154.2 55.2 reduce-scatter.3
  254.5 34.1 all-gather.34
  290.9 29.3 all-gather.22
  322.4 33.2 all-gather.36
  358.1 29.3 all-gather.24
  391.7 33.2 all-gather.42
  426.9 29.3 all-gather.26
  458.3 33.2 all-gather.40
  493.4 29.3 all-gather.28
  524.8 33.2 all-gather.38
  560.5 29.3 all-gather.30
  593.7 30.3 all-gather.32
where the time goes:
time: 641 us; the launch traced here: 640 us
  waiting for transfers between devices  508 us (79%)
  matrix products  47.6 us (7%)
  blocking collectives  39.5 us (6%)
  between operations  16.7 us (3%)
  local copies, waits for them, and re-layouts  15.4 us (2%)
  other arithmetic  12.4 us (2%)
    all_gather x5, waiting for transfers between devices, multiply(): left_rows = lax.all_gather(left_low, 'fs', axis=1, tiled=True)  155 us
    all_gather x5, waiting for transfers between devices, multiply(): lax.all_gather(right_low, 'tp', axis=0, tiled=True)  143 us
    all_gather x1, waiting for transfers between devices, local(): lax.all_gather(low_gate, 'fs', axis=0, tiled=True)  63.8 us
    all_gather x1, waiting for transfers between devices, local(): lax.all_gather(low_up, 'fs', axis=0, tiled=True)  58.9 us
    unnamed x15, waiting for transfers between devices  56.5 us
    psum x1, blocking collectives, local(): lax.psum((trace_local, square_local), ('fs', 'tp'))  39.5 us
    all_gather x1, waiting for transfers between devices, local(): segment = lax.all_gather(product_low, 'tp', axis=0, tiled=True)  30.4 us
    dot_general x6, matrix products, multiply(): jnp.dot(left_rows, lax.all_gather(right_low, 'tp', axis=0, tiled=True), p...  22.6 us
  transfers between devices with their start and end apart: 14, of which 14 were waited for; matrix products, arithmetic and copies ran while one was open for 6% of the time, Pallas kernels for 0%

commit v1 on v0

--- a/solution.py
+++ b/solution.py
@@ -10,7 +10,12 @@
 
 
 def multiply(left_low, right_low):
-    left_rows = lax.all_gather(left_low, "fs", axis=1, tiled=True)
+    ring = [left_low]
+    for hop in range(3):
+        ring.append(lax.ppermute(ring[-1], "fs", [(dev, (dev + 1) % 4) for dev in range(4)]))
+    left_rows = jnp.roll(
+        jnp.concatenate(ring[::-1], axis=1), (lax.axis_index("fs") + 1) * ring[0].shape[1], axis=1
+    )
     return jnp.dot(
         left_rows,
         lax.all_gather(right_low, "tp", axis=0, tiled=True),

time: 641 us -> 480 us (0.75)
  waiting for transfers between devices: 508 us -> 347 us
    all_gather x5 -> x0, waiting for transfers between devices: 155 us -> none  [multiply(): left_rows = lax.all_gather(left_low, 'fs', axis=1, tiled=True)]
    all_gather x5, waiting for transfers between devices: 143 us -> 0.11 us  [multiply(): lax.all_gather(right_low, 'tp', axis=0, tiled=True)]
    ppermute x0 -> x15, waiting for transfers between devices: none -> 141 us  [multiply(): lax.ppermute(ring[-1], 'fs', [(dev, (dev + 1) % 4) for dev in range(4)])]
    concatenate x0 -> x5, local copies, waits for them, and re-layouts: none -> 10.3 us  [multiply(): jnp.concatenate(ring[::-1], axis=1)]
    all_gather x5 -> x0, local copies, waits for them, and re-layouts: 9.26 us -> none  [multiply(): left_rows = lax.all_gather(left_low, 'fs', axis=1, tiled=True)]
    unnamed x15 -> x10, waiting for transfers between devices: 56.5 us -> 54.2 us
  transfers between devices with their start and end apart: 14 -> 24, of which waited for: 14 -> 19; matrix products, arithmetic and copies ran while one was open for 6% -> 5% of each run, Pallas kernels for 0% -> 0%
where the time goes in v1:
time: 480 us; the launch traced here: 479 us
  waiting for transfers between devices  347 us (72%)
  matrix products  51.1 us (11%)
  blocking collectives  39.5 us (8%)
  between operations  16.8 us (4%)
  other arithmetic  12.3 us (3%)
  local copies, waits for them, and re-layouts  10.3 us (2%)
    ppermute x15, waiting for transfers between devices, multiply(): lax.ppermute(ring[-1], 'fs', [(dev, (dev + 1) % 4) for dev in range(4)])  141 us
    all_gather x1, waiting for transfers between devices, local(): lax.all_gather(low_gate, 'fs', axis=0, tiled=True)  63.8 us
    all_gather x1, waiting for transfers between devices, local(): lax.all_gather(low_up, 'fs', axis=0, tiled=True)  58.8 us
    unnamed x10, waiting for transfers between devices  54.2 us
    psum x1, blocking collectives, local(): lax.psum((trace_local, square_local), ('fs', 'tp'))  39.5 us
    all_gather x1, waiting for transfers between devices, local(): segment = lax.all_gather(product_low, 'tp', axis=0, tiled=True)  28.4 us
    dot_general x6, matrix products, multiply(): jnp.dot(left_rows, lax.all_gather(right_low, 'tp', axis=0, tiled=True), p...  26 us
    concatenate x5, local copies, waits for them, and re-layouts, multiply(): jnp.concatenate(ring[::-1], axis=1)  10.3 us
  transfers between devices with their start and end apart: 24, of which 19 were waited for; matrix products, arithmetic and copies ran while one was open for 5% of the time, Pallas kernels for 0%

profile of v1, /device:TPU:0, one launch (start us, length us, event | category | flops | bytes accessed | tf_op | source)
XLA Modules:
  0.0 479.0 jit_solution(15664307501275734671)
XLA Ops:
  7.2 4.5 multiply_reduce_fusion.1
  11.8 4.0 multiply_reduce_fusion
  15.8 63.8 %all-gather.9.cloned.1.call-done = bf16[2112,704]{1,0:T(8,128)(2,1)} async-done(((bf16[528,704]{1,0:T(8,128)(2,1)}), bf16[2112,704]{1,0:T(8,128)(2,1)}) %all-gather.9.cloned.1.call-update) | async-done | bytes 2973712 | tf_op jit(solution)/shard_map/all_gather | solution.py:35
  79.6 7.0 %fusion.26 = f32[2112,528]{1,0:T(8,128)} fusion(bf16[2112,704]{1,0:T(8,128)(2,1)} %all-gather.9.cloned.1.call-done, bf16[528,704]{1,0:T(8,128)(2,1)S(1)} %copy-done), kind=kOutput, calls=%fused_computation.48 | convolution fusion | flops 1570111488 | bytes 8177664 | tf_op jit(solution)/shard_map/ik,jk->ij/dot_general | solution.py:44
  86.7 58.8 %all-gather.11.cloned.1.call-done = bf16[2112,704]{1,0:T(8,128)(2,1)} async-done(((bf16[528,704]{1,0:T(8,128)(2,1)}), bf16[2112,704]{1,0:T(8,128)(2,1)}) %all-gather.11.cloned.1.call-update) | async-done | bytes 2973712 | tf_op jit(solution)/shard_map/all_gather | solution.py:36
  145.5 8.6 %convolution_add_fusion = f32[2112,528]{1,0:T(8,128)} fusion(f32[2112,528]{1,0:T(8,128)} %fusion.26, bf16[2112,704]{1,0:T(8,128)(2,1)} %all-gather.11.cloned.1.call-done, bf16[528,704]{1,0:T(8,128)(2,1)S(1)} %copy-done.1), kind=kOutput, calls=%fused_computation | convolution fusion | flops 1571226624 | bytes 12638208 | tf_op jit(solution)/shard_map/ik,jk->ij/dot_general | solution.py:45
  155.5 54.0 %reduce-scatter.4.cloned.1.call-done = f32[264,528]{1,0:T(8,128)} async-done(((f32[2112,528]{1,0:T(8,128)}), f32[264,528]{1,0:T(8,128)}) %reduce-scatter.4.cloned.1.call-update) | async-done | bytes 557584
  211.5 39.5 %all-reduce.1 = (f32[]{:T(128)}, f32[]{:T(128)}) all-reduce(f32[]{:T(128)} %multiply_reduce_fusion.2, f32[]{:T(128)S(6)} %add.58), channel_id=1, replica_groups=mesh['fs'=4,'tp'=8] {'fs','tp'}, use_global_device_ids=true, to_apply=%region_2.0 | all-reduce | flops 2 | bytes 16 | tf_op jit(solution)/shard_map/psum | solution.py:51
  255.9 9.6 %collective-permute-done = bf16[264,528]{1,0:T(8,128)(2,1)S(1)} collective-permute-done((bf16[264,528]{1,0:T(8,128)(2,1)}, bf16[264,528]{1,0:T(8,128)(2,1)S(1)}, u32[]{:S(2)}, u32[]{:S(2)}) %collective-permute-start) | collective-permute-done | bytes 278816 | tf_op jit(solution)/shard_map/ppermute | solution.py:15
  265.5 10.0 %collective-permute-done.1 = bf16[264,528]{1,0:T(8,128)(2,1)S(1)} collective-permute-done((bf16[264,528]{1,0:T(8,128)(2,1)S(1)}, bf16[264,528]{1,0:T(8,128)(2,1)S(1)}, u32[]{:S(2)}, u32[]{:S(2)}) %collective-permute-start.1) | collective-permute-done | bytes 278816 | tf_op jit(solution)/shard_map/ppermute | solution.py:15
  275.4 9.1 %collective-permute-done.2 = bf16[264,528]{1,0:T(8,128)(2,1)S(1)} collective-permute-done((bf16[264,528]{1,0:T(8,128)(2,1)S(1)}, bf16[264,528]{1,0:T(8,128)(2,1)S(1)}, u32[]{:S(2)}, u32[]{:S(2)}) %collective-permute-start.2) | collective-permute-done | bytes 278816 | tf_op jit(solution)/shard_map/ppermute | solution.py:15
  287.0 4.4 convolution_convert_fusion.3
  291.8 10.4 %collective-permute-done.3 = bf16[264,528]{1,0:T(8,128)(2,1)S(1)} collective-permute-done((bf16[264,528]{1,0:T(8,128)(2,1)S(1)}, bf16[264,528]{1,0:T(8,128)(2,1)S(1)}, u32[]{:S(2)}, u32[]{:S(2)}) %collective-permute-start.3) | collective-permute-done | bytes 278816 | tf_op jit(solution)/shard_map/ppermute | solution.py:15
  302.1 9.7 %collective-permute-done.4 = bf16[264,528]{1,0:T(8,128)(2,1)S(1)} collective-permute-done((bf16[264,528]{1,0:T(8,128)(2,1)S(1)}, bf16[264,528]{1,0:T(8,128)(2,1)S(1)}, u32[]{:S(2)}, u32[]{:S(2)}) %collective-permute-start.4) | collective-permute-done | bytes 278816 | tf_op jit(solution)/shard_map/ppermute | solution.py:15
  311.9 9.1 %collective-permute-done.5 = bf16[264,528]{1,0:T(8,128)(2,1)} collective-permute-done((bf16[264,528]{1,0:T(8,128)(2,1)S(1)}, bf16[264,528]{1,0:T(8,128)(2,1)}, u32[]{:S(2)}, u32[]{:S(2)}) %collective-permute-start.5) | collective-permute-done | bytes 278816 | tf_op jit(solution)/shard_map/ppermute | solution.py:15
  323.3 4.5 fusion.25
  327.9 9.4 %collective-permute-done.12 = bf16[264,528]{1,0:T(8,128)(2,1)S(1)} collective-permute-done((bf16[264,528]{1,0:T(8,128)(2,1)}, bf16[264,528]{1,0:T(8,128)(2,1)S(1)}, u32[]{:S(2)}, u32[]{:S(2)}) %collective-permute-start.12) | collective-permute-done | bytes 278816 | tf_op jit(solution)/shard_map/ppermute | solution.py:15
  337.3 9.0 %collective-permute-done.13 = bf16[264,528]{1,0:T(8,128)(2,1)S(1)} collective-permute-done((bf16[264,528]{1,0:T(8,128)(2,1)S(1)}, bf16[264,528]{1,0:T(8,128)(2,1)S(1)}, u32[]{:S(2)}, u32[]{:S(2)}) %collective-permute-start.13) | collective-permute-done | bytes 278816 | tf_op jit(solution)/shard_map/ppermute | solution.py:15
  346.3 9.1 %collective-permute-done.14 = bf16[264,528]{1,0:T(8,128)(2,1)} collective-permute-done((bf16[264,528]{1,0:T(8,128)(2,1)S(1)}, bf16[264,528]{1,0:T(8,128)(2,1)}, u32[]{:S(2)}, u32[]{:S(2)}) %collective-permute-start.14) | collective-permute-done | bytes 278816 | tf_op jit(solution)/shard_map/ppermute | solution.py:15
  357.8 4.4 convolution_convert_fusion.1
  362.4 10.1 %collective-permute-done.9 = bf16[264,528]{1,0:T(8,128)(2,1)S(1)} collective-permute-done((bf16[264,528]{1,0:T(8,128)(2,1)S(1)}, bf16[264,528]{1,0:T(8,128)(2,1)S(1)}, u32[]{:S(2)}, u32[]{:S(2)}) %collective-permute-start.9) | collective-permute-done | bytes 278816 | tf_op jit(solution)/shard_map/ppermute | solution.py:15
  372.5 9.2 %collective-permute-done.10 = bf16[264,528]{1,0:T(8,128)(2,1)S(1)} collective-permute-done((bf16[264,528]{1,0:T(8,128)(2,1)S(1)}, bf16[264,528]{1,0:T(8,128)(2,1)S(1)}, u32[]{:S(2)}, u32[]{:S(2)}) %collective-permute-start.10) | collective-permute-done | bytes 278816 | tf_op jit(solution)/shard_map/ppermute | solution.py:15
  381.7 9.1 %collective-permute-done.11 = bf16[264,528]{1,0:T(8,128)(2,1)} collective-permute-done((bf16[264,528]{1,0:T(8,128)(2,1)S(1)}, bf16[264,528]{1,0:T(8,128)(2,1)}, u32[]{:S(2)}, u32[]{:S(2)}) %collective-permute-start.11) | collective-permute-done | bytes 278816 | tf_op jit(solution)/shard_map/ppermute | solution.py:15
  393.1 4.5 fusion.1
  397.7 3.7 convolution_convert_fusion.2
  401.4 9.7 %collective-permute-done.6 = bf16[264,528]{1,0:T(8,128)(2,1)S(1)} collective-permute-done((bf16[264,528]{1,0:T(8,128)(2,1)S(1)}, bf16[264,528]{1,0:T(8,128)(2,1)S(1)}, u32[]{:S(2)}, u32[]{:S(2)}) %collective-permute-start.6) | collective-permute-done | bytes 278816 | tf_op jit(solution)/shard_map/ppermute | solution.py:15
  411.1 9.1 %collective-permute-done.7 = bf16[264,528]{1,0:T(8,128)(2,1)S(1)} collective-permute-done((bf16[264,528]{1,0:T(8,128)(2,1)S(1)}, bf16[264,528]{1,0:T(8,128)(2,1)S(1)}, u32[]{:S(2)}, u32[]{:S(2)}) %collective-permute-start.7) | collective-permute-done | bytes 278816 | tf_op jit(solution)/shard_map/ppermute | solution.py:15
  420.2 9.0 %collective-permute-done.8 = bf16[264,528]{1,0:T(8,128)(2,1)S(1)} collective-permute-done((bf16[264,528]{1,0:T(8,128)(2,1)S(1)}, bf16[264,528]{1,0:T(8,128)(2,1)S(1)}, u32[]{:S(2)}, u32[]{:S(2)}) %collective-permute-start.8) | collective-permute-done | bytes 278816 | tf_op jit(solution)/shard_map/ppermute | solution.py:15
  430.1 4.4 convolution_convert_fusion
  434.7 28.4 %all-gather.23.cloned.1.call-done = bf16[2112,528]{1,0:T(8,128)(2,1)} async-done(((bf16[264,528]{1,0:T(8,128)(2,1)}), bf16[2112,528]{1,0:T(8,128)(2,1)}) %all-gather.23.cloned.1.call-update) | async-done | bytes 2230288 | tf_op jit(solution)/shard_map/all_gather | solution.py:77
  463.1 6.1 %convolution_multiply_fusion = f32[528,704]{1,0:T(8,128)} fusion(bf16[2112,528]{1,0:T(8,128)(2,1)} %all-gather.23.cloned.1.call-done, bf16[2112,704]{1,0:T(8,128)(2,1)} %all-gather.11.cloned.1.call-done, f32[]{:T(128)S(6)} %sqrt.3), kind=kOutput, calls=%fused_computation.15 | convolution fusion | flops 1570483200 | bytes 6690820 | tf_op jit(solution)/shard_map/jr,jc->rc/dot_general | solution.py:81
  469.2 3.3 convolution_multiply_fusion.1
  (57 shorter events, 16.8 us)
Async XLA Ops:
  7.2 4.6 copy-start.2
  7.2 72.5 %all-gather.9.cloned.1.call-start = ((), (), s32[]{:S(2)}) async-start(), calls=%async_computation.1 | async-start | bytes 4055040 | tf_op jit(solution)/shard_map/all_gather | solution.py:35
  11.7 67.9 %copy-start = (bf16[528,704]{1,0:T(8,128)(2,1)S(1)}, bf16[528,704]{1,0:T(8,128)(2,1)}, u32[]{:S(2)}) copy-start(bf16[528,704]{1,0:T(8,128)(2,1)} %get-tuple-element.11) | copy-start | bytes 2230276
  11.7 133.8 %all-gather.11.cloned.1.call-start = ((), (), s32[]{:S(2)}) async-start(), calls=%async_computation.2 | async-start | bytes 4055040 | tf_op jit(solution)/shard_map/all_gather | solution.py:36
  15.8 129.8 %copy-start.1 = (bf16[528,704]{1,0:T(8,128)(2,1)S(1)}, bf16[528,704]{1,0:T(8,128)(2,1)}, u32[]{:S(2)}) copy-start(bf16[528,704]{1,0:T(8,128)(2,1)} %get-tuple-element.8) | copy-start | bytes 2230276
  15.8 193.8 %reduce-scatter.4.cloned.1.call-start = ((), (), s32[]{:S(2)}) async-start(), calls=%async_computation.9 | async-start | bytes 6082560
  154.2 132.8 %all-gather.13.cloned.1.call-start = ((), (), s32[]{:S(2)}) async-start(), calls=%async_computation.3 | async-start | bytes 3041280 | tf_op jit(solution)/shard_map/all_gather | solution.py:21
  254.3 69.0 %all-gather.15.cloned.1.call-start = ((), (), s32[]{:S(2)}) async-start(), calls=%async_computation.4 | async-start | bytes 3041280 | tf_op jit(solution)/shard_map/all_gather | solution.py:21
  254.4 11.1 %collective-permute-start = (bf16[264,528]{1,0:T(8,128)(2,1)}, bf16[264,528]{1,0:T(8,128)(2,1)S(1)}, u32[]{:S(2)}, u32[]{:S(2)}) collective-permute-start(bf16[264,528]{1,0:T(8,128)(2,1)} %get-tuple-element.16), channel_id=1, source_target_pairs={{0,8},{8,16},{16,24},{24,0},{1,9},{9,17},{17,25},{25,1},{2,10},{10... | collective-permute-start | bytes 836360 | tf_op jit(solution)/shard_map/ppermute | solution.py:15
  265.5 10.0 %collective-permute-start.1 = (bf16[264,528]{1,0:T(8,128)(2,1)S(1)}, bf16[264,528]{1,0:T(8,128)(2,1)S(1)}, u32[]{:S(2)}, u32[]{:S(2)}) collective-permute-start(bf16[264,528]{1,0:T(8,128)(2,1)S(1)} %collective-permute-done), channel_id=1, source_target_pairs={{0,8},{8,16},{16,24},{24,0},{1,9},{9,17},{17,25},{25,1},{2,10},{10... | collective-permute-start | bytes 836360 | tf_op jit(solution)/shard_map/ppermute | solution.py:15
  275.4 9.1 %collective-permute-start.2 = (bf16[264,528]{1,0:T(8,128)(2,1)S(1)}, bf16[264,528]{1,0:T(8,128)(2,1)S(1)}, u32[]{:S(2)}, u32[]{:S(2)}) collective-permute-start(bf16[264,528]{1,0:T(8,128)(2,1)S(1)} %collective-permute-done.1), channel_id=1, source_target_pairs={{0,8},{8,16},{16,24},{24,0},{1,9},{9,17},{17,25},{25,1},{2,10},{10... | collective-permute-start | bytes 836360 | tf_op jit(solution)/shard_map/ppermute | solution.py:15
  291.4 66.4 %all-gather.17.cloned.1.call-start = ((), (), s32[]{:S(2)}) async-start(), calls=%async_computation.5 | async-start | bytes 3041280 | tf_op jit(solution)/shard_map/all_gather | solution.py:21
  291.5 10.7 %collective-permute-start.3 = (bf16[264,528]{1,0:T(8,128)(2,1)S(1)}, bf16[264,528]{1,0:T(8,128)(2,1)S(1)}, u32[]{:S(2)}, u32[]{:S(2)}) collective-permute-start(bf16[264,528]{1,0:T(8,128)(2,1)S(1)} %get-tuple-element.15), channel_id=1, source_target_pairs={{0,8},{8,16},{16,24},{24,0},{1,9},{9,17},{17,25},{25,1},{2,10},{10... | collective-permute-start | bytes 836360 | tf_op jit(solution)/shard_map/ppermute | solution.py:15
  302.1 9.7 %collective-permute-start.4 = (bf16[264,528]{1,0:T(8,128)(2,1)S(1)}, bf16[264,528]{1,0:T(8,128)(2,1)S(1)}, u32[]{:S(2)}, u32[]{:S(2)}) collective-permute-start(bf16[264,528]{1,0:T(8,128)(2,1)S(1)} %collective-permute-done.3), channel_id=1, source_target_pairs={{0,8},{8,16},{16,24},{24,0},{1,9},{9,17},{17,25},{25,1},{2,10},{10... | collective-permute-start | bytes 836360 | tf_op jit(solution)/shard_map/ppermute | solution.py:15
  311.9 9.1 %collective-permute-start.5 = (bf16[264,528]{1,0:T(8,128)(2,1)S(1)}, bf16[264,528]{1,0:T(8,128)(2,1)}, u32[]{:S(2)}, u32[]{:S(2)}) collective-permute-start(bf16[264,528]{1,0:T(8,128)(2,1)S(1)} %collective-permute-done.4), channel_id=1, source_target_pairs={{0,8},{8,16},{16,24},{24,0},{1,9},{9,17},{17,25},{25,1},{2,10},{10... | collective-permute-start | bytes 836360 | tf_op jit(solution)/shard_map/ppermute | solution.py:15
  327.8 65.3 %all-gather.19.cloned.1.call-start = ((), (), s32[]{:S(2)}) async-start(), calls=%async_computation.6 | async-start | bytes 3041280 | tf_op jit(solution)/shard_map/all_gather | solution.py:21
  327.9 9.5 %collective-permute-start.12 = (bf16[264,528]{1,0:T(8,128)(2,1)}, bf16[264,528]{1,0:T(8,128)(2,1)S(1)}, u32[]{:S(2)}, u32[]{:S(2)}) collective-permute-start(bf16[264,528]{1,0:T(8,128)(2,1)} %get-tuple-element.14), channel_id=1, source_target_pairs={{0,8},{8,16},{16,24},{24,0},{1,9},{9,17},{17,25},{25,1},{2,10},{10... | collective-permute-start | bytes 836360 | tf_op jit(solution)/shard_map/ppermute | solution.py:15
  337.3 9.0 %collective-permute-start.13 = (bf16[264,528]{1,0:T(8,128)(2,1)S(1)}, bf16[264,528]{1,0:T(8,128)(2,1)S(1)}, u32[]{:S(2)}, u32[]{:S(2)}) collective-permute-start(bf16[264,528]{1,0:T(8,128)(2,1)S(1)} %collective-permute-done.12), channel_id=1, source_target_pairs={{0,8},{8,16},{16,24},{24,0},{1,9},{9,17},{17,25},{25,1},{2,10},{10... | collective-permute-start | bytes 836360 | tf_op jit(solution)/shard_map/ppermute | solution.py:15
  346.3 9.1 %collective-permute-start.14 = (bf16[264,528]{1,0:T(8,128)(2,1)S(1)}, bf16[264,528]{1,0:T(8,128)(2,1)}, u32[]{:S(2)}, u32[]{:S(2)}) collective-permute-start(bf16[264,528]{1,0:T(8,128)(2,1)S(1)} %collective-permute-done.13), channel_id=1, source_target_pairs={{0,8},{8,16},{16,24},{24,0},{1,9},{9,17},{17,25},{25,1},{2,10},{10... | collective-permute-start | bytes 836360 | tf_op jit(solution)/shard_map/ppermute | solution.py:15
  362.3 67.8 %all-gather.21.cloned.1.call-start = ((), (), s32[]{:S(2)}) async-start(), calls=%async_computation.7 | async-start | bytes 3041280 | tf_op jit(solution)/shard_map/all_gather | solution.py:21
  362.4 10.1 %collective-permute-start.9 = (bf16[264,528]{1,0:T(8,128)(2,1)S(1)}, bf16[264,528]{1,0:T(8,128)(2,1)S(1)}, u32[]{:S(2)}, u32[]{:S(2)}) collective-permute-start(bf16[264,528]{1,0:T(8,128)(2,1)S(1)} %get-tuple-element.13), channel_id=1, source_target_pairs={{0,8},{8,16},{16,24},{24,0},{1,9},{9,17},{17,25},{25,1},{2,10},{10... | collective-permute-start | bytes 836360 | tf_op jit(solution)/shard_map/ppermute | solution.py:15
  372.5 9.2 %collective-permute-start.10 = (bf16[264,528]{1,0:T(8,128)(2,1)S(1)}, bf16[264,528]{1,0:T(8,128)(2,1)S(1)}, u32[]{:S(2)}, u32[]{:S(2)}) collective-permute-start(bf16[264,528]{1,0:T(8,128)(2,1)S(1)} %collective-permute-done.9), channel_id=1, source_target_pairs={{0,8},{8,16},{16,24},{24,0},{1,9},{9,17},{17,25},{25,1},{2,10},{10... | collective-permute-start | bytes 836360 | tf_op jit(solution)/shard_map/ppermute | solution.py:15
  381.7 9.1 %collective-permute-start.11 = (bf16[264,528]{1,0:T(8,128)(2,1)S(1)}, bf16[264,528]{1,0:T(8,128)(2,1)}, u32[]{:S(2)}, u32[]{:S(2)}) collective-permute-start(bf16[264,528]{1,0:T(8,128)(2,1)S(1)} %collective-permute-done.10), channel_id=1, source_target_pairs={{0,8},{8,16},{16,24},{24,0},{1,9},{9,17},{17,25},{25,1},{2,10},{10... | collective-permute-start | bytes 836360 | tf_op jit(solution)/shard_map/ppermute | solution.py:15
  397.6 65.5 %all-gather.23.cloned.1.call-start = ((), (), s32[]{:S(2)}) async-start(), calls=%async_computation.8 | async-start | bytes 3041280 | tf_op jit(solution)/shard_map/all_gather | solution.py:77
  401.4 9.7 %collective-permute-start.6 = (bf16[264,528]{1,0:T(8,128)(2,1)S(1)}, bf16[264,528]{1,0:T(8,128)(2,1)S(1)}, u32[]{:S(2)}, u32[]{:S(2)}) collective-permute-start(bf16[264,528]{1,0:T(8,128)(2,1)S(1)} %convolution_convert_fusion.2), channel_id=1, source_target_pairs={{0,8},{8,16},{16,24},{24,0},{1,9},{9,17},{17,25},{25,1},{2,10},{10... | collective-permute-start | bytes 836360 | tf_op jit(solution)/shard_map/ppermute | solution.py:15
  411.1 9.1 %collective-permute-start.7 = (bf16[264,528]{1,0:T(8,128)(2,1)S(1)}, bf16[264,528]{1,0:T(8,128)(2,1)S(1)}, u32[]{:S(2)}, u32[]{:S(2)}) collective-permute-start(bf16[264,528]{1,0:T(8,128)(2,1)S(1)} %collective-permute-done.6), channel_id=1, source_target_pairs={{0,8},{8,16},{16,24},{24,0},{1,9},{9,17},{17,25},{25,1},{2,10},{10... | collective-permute-start | bytes 836360 | tf_op jit(solution)/shard_map/ppermute | solution.py:15
  420.2 9.0 %collective-permute-start.8 = (bf16[264,528]{1,0:T(8,128)(2,1)S(1)}, bf16[264,528]{1,0:T(8,128)(2,1)S(1)}, u32[]{:S(2)}, u32[]{:S(2)}) collective-permute-start(bf16[264,528]{1,0:T(8,128)(2,1)S(1)} %collective-permute-done.7), channel_id=1, source_target_pairs={{0,8},{8,16},{16,24},{24,0},{1,9},{9,17},{17,25},{25,1},{2,10},{10... | collective-permute-start | bytes 836360 | tf_op jit(solution)/shard_map/ppermute | solution.py:15
  434.7 34.5 %copy-start.3 = (bf16[2112,704]{1,0:T(8,128)(2,1)S(1)}, bf16[2112,704]{1,0:T(8,128)(2,1)}, u32[]{:S(2)}) copy-start(bf16[2112,704]{1,0:T(8,128)(2,1)} %all-gather.9.cloned.1.call-done) | copy-start | bytes 8921092
  463.1 6.1 %copy-start.4 = (bf16[2112,528]{1,0:T(8,128)(2,1)S(1)}, bf16[2112,528]{1,0:T(8,128)(2,1)}, u32[]{:S(2)}) copy-start(bf16[2112,528]{1,0:T(8,128)(2,1)} %all-gather.23.cloned.1.call-done) | copy-start | bytes 6690820
Sparse Core Ops, SparseCore 0:
  11.8 67.7 all-gather.8
  81.8 63.6 all-gather.10
  154.3 55.2 reduce-scatter.3
  254.4 31.2 all-gather.12
  291.6 29.0 all-gather.14
  327.9 28.0 all-gather.16
  362.4 28.4 all-gather.18
  397.7 28.0 all-gather.20
  434.7 28.3 all-gather.22
